TPU v7x, 32 devices: a whole 2x2x4 slice. The times are simulated.
32 devices in a mesh: tp: 8 (over z, core), dp: 4 (over y, x).
Axes of the slice: x: 2, y: 2, z: 4, core: 2. Of those that a mesh axis runs over, the one named last changes fastest.
Arguments:
- tokens: bfloat16 [128, 2048], P(None, 'dp'), may hold values from -21 to 21
- lengths: int32 [8], P('dp'), may hold values from 1 to 16, 42 in all
- input_norm_scale: float32 [2, 2048], P(None, 'dp'), may hold values from 0.1 to 1.9
- gate_input_weight: bfloat16 [2, 2048, 2, 2048], P(None, 'dp', None, 'tp'), may hold values from -0.125 to 0.125
- maps_weight: bfloat16 [2, 2048, 2, 512], P(None, 'dp', None, 'tp'), may hold values from -0.125 to 0.125
- step_weight: bfloat16 [2, 2048, 32], P(None, 'dp', 'tp'), may hold values from -0.125 to 0.125
- input_tap_weight: bfloat16 [2, 4, 2048], P(None, None, 'tp'), may hold values from -3 to 3
- map_tap_weight: bfloat16 [2, 4, 2, 512], P(None, None, None, 'tp'), may hold values from -3 to 3
- step_size_bias: float32 [2, 32], P(None, 'tp'), may hold values from -4 to -1
- decay_rate_logarithm: float32 [2, 32], P(None, 'tp'), may hold values from -2 to 2.5
- direct_path_weight: float32 [2, 32], P(None, 'tp'), may hold values from 0.25 to 2.5
- head_norm_scale: float32 [2, 2048], P(None, 'tp'), may hold values from 0.1 to 1.9
- output_weight: bfloat16 [2, 2048, 2048], P(None, 'tp', 'dp'), may hold values from -0.125 to 0.125
- convolution_input_cache: bfloat16 [2, 8, 3, 2048], P(None, 'dp', None, 'tp'), may hold values from -6 to 6
- convolution_map_cache: bfloat16 [2, 8, 3, 2, 512], P(None, 'dp', None, None, 'tp'), may hold values from -6 to 6
- recurrent_state: float32 [2, 8, 32, 64, 128], P(None, 'dp', 'tp'), may hold values from -6 to 6
- extra_log_decay: float32 [2, 8, 16, 32], P(None, 'dp', None, 'tp'), may hold values from -0.7 to 0, as said below
Outputs:
- stream_out: float32 [128, 2048], P(None, 'dp')
- conv_input_out: bfloat16 [2, 8, 3, 2048], P(None, 'dp', None, 'tp')
- conv_maps_out: bfloat16 [2, 8, 3, 2, 512], P(None, 'dp', None, None, 'tp')
- ssm_out: float32 [2, 8, 32, 64, 128], P(None, 'dp', 'tp')
Inputs may be any that keep to these rules, and one draw needn't show every extreme that they name: `extra_log_decay`: zero at most slots, a drop of a fifth to a half of the state at a few.
All inputs are finite; a program needn't handle non-finite values. No bound on the sum of `lengths` on one device may be relied on, other than what follows from the above.
Results may differ from a plain program's by a relative error of at most 0.04.
Values may be sent and summed in bfloat16 or wider, within the bound.
A program may use at most 64 MiB of HBM per device.

v0:
```python
import jax
import jax.numpy as jnp
from jax import lax
from jax.sharding import PartitionSpec as P

D = 2048
STATE_HEADS = 32
N = 128
G = 4
MIXER_LAYERS = 2


epsilon = 1e-06
highest = lax.Precision.HIGHEST


def conv_step(previous, incoming, weights, lengths):
    padded = jnp.concatenate([previous, incoming], axis=1).astype(jnp.float32)
    taps = weights.shape[0]
    fresh_tokens = incoming.shape[1]
    filtered = padded[:, :fresh_tokens] * weights[0].astype(jnp.float32)
    for tap_index in range(1, taps):
        filtered = filtered + padded[:, tap_index : tap_index + fresh_tokens] * weights[
            tap_index
        ].astype(jnp.float32)
    position = jnp.arange(fresh_tokens + taps - 1, dtype=jnp.int32)
    wanted = lengths[:, None] + jnp.arange(taps - 1, dtype=jnp.int32)[None, :]
    chooser = (position[None, None, :] == wanted[:, :, None]).astype(jnp.float32)
    kept_rows = jnp.einsum("skp,sp...->sk...", chooser, padded, precision=highest)
    return (jax.nn.silu(filtered), kept_rows.astype(jnp.bfloat16))


def ssd_block(
    head_input,
    head_gate,
    head_step_size,
    decay_logarithm,
    write_map,
    read_map,
    state_old,
    skip,
    gain_heads,
):
    decay_sum = jnp.cumsum(decay_logarithm, axis=1)
    slots = decay_logarithm.shape[1]
    causal = jnp.arange(slots)[:, None] >= jnp.arange(slots)[None, :]
    decay_gap = decay_sum[:, :, None, :] - decay_sum[:, None, :, :]
    segment = jnp.exp(jnp.where(causal[None, :, :, None], decay_gap, -jnp.inf))
    intersection = jnp.einsum("slhn,smhn->slmh", read_map, write_map, precision=highest)
    within = jnp.einsum(
        "slmh,smh,smhp->slhp", intersection * segment, head_step_size, head_input, precision=highest
    )
    carried = (
        jnp.einsum("slhn,shpn->slhp", read_map, state_old, precision=highest)
        * jnp.exp(decay_sum)[..., None]
    )
    to_end = jnp.exp(decay_sum[:, -1:, :] - decay_sum)
    state_new = jnp.exp(decay_sum[:, -1])[..., None, None] * state_old + jnp.einsum(
        "smhn,smh,smhp->shpn", write_map, to_end * head_step_size, head_input, precision=highest
    )
    mixed_out = within + carried + skip[:, None] * head_input
    mixed_out = mixed_out * jax.nn.silu(head_gate)
    mixed_out = (
        mixed_out
        * lax.rsqrt(jnp.mean(mixed_out * mixed_out, axis=-1, keepdims=True) + epsilon)
        * gain_heads
    )
    return (mixed_out, state_new)


def body(
    tokens,
    lengths,
    input_norm_scale,
    gate_input_weight,
    maps_weight,
    step_weight,
    input_tap_weight,
    map_tap_weight,
    step_size_bias,
    decay_rate_logarithm,
    direct_path_weight,
    head_norm_scale,
    output_weight,
    convolution_input_cache,
    convolution_map_cache,
    recurrent_state,
    extra_log_decay,
):
    head_rank = lax.axis_index("tp")
    seq_rank = lax.axis_index("dp")
    local_sequences = extra_log_decay.shape[1]
    fresh_tokens = extra_log_decay.shape[2]
    heads_here = step_size_bias.shape[1]
    head_size = head_norm_scale.shape[1] // heads_here
    own_rows = local_sequences * fresh_tokens
    active_mask = (jnp.arange(fresh_tokens, dtype=jnp.int32)[None, :] < lengths[:, None]).astype(
        jnp.float32
    )
    group_index = head_rank * heads_here // (STATE_HEADS // G)
    stream = tokens.astype(jnp.float32)
    input_states, map_states, ssm_states = ([], [], [])
    for layer_number in range(MIXER_LAYERS):
        stream_f = stream
        row_squares = jnp.sum(stream_f * stream_f, axis=1)
        normed = (stream_f * input_norm_scale[layer_number]).astype(jnp.bfloat16)
        pair_partial = jnp.einsum(
            "td,dkc->tkc",
            normed,
            gate_input_weight[layer_number],
            preferred_element_type=jnp.float32,
        )
        maps_partial = jnp.einsum(
            "td,dkc->tkc", normed, maps_weight[layer_number], preferred_element_type=jnp.float32
        )
        step_partial = jnp.dot(
            normed, step_weight[layer_number], preferred_element_type=jnp.float32
        )
        squares = lax.psum(row_squares, "dp")
        factor = lax.rsqrt(squares / D + epsilon)
        own_factor = lax.dynamic_slice_in_dim(factor, seq_rank * own_rows, own_rows)[:, None]
        pair_sum, maps_sum, step_sum = (
            lax.psum_scatter(
                pair_partial.astype(jnp.bfloat16), "dp", scatter_dimension=0, tiled=True
            ).astype(jnp.float32),
            lax.psum_scatter(
                maps_partial.astype(jnp.bfloat16), "dp", scatter_dimension=0, tiled=True
            ).astype(jnp.float32),
            lax.psum_scatter(
                step_partial.astype(jnp.bfloat16), "dp", scatter_dimension=0, tiled=True
            ).astype(jnp.float32),
        )
        gate_input = (
            (pair_sum * own_factor[:, :, None])
            .astype(jnp.bfloat16)
            .reshape(local_sequences, fresh_tokens, 2, pair_sum.shape[2])
        )
        map_input = (
            (maps_sum * own_factor[:, :, None])
            .astype(jnp.bfloat16)
            .reshape(local_sequences, fresh_tokens, 2, maps_sum.shape[2])
        )
        step_raw = (
            (step_sum * own_factor)
            .astype(jnp.bfloat16)
            .reshape(local_sequences, fresh_tokens, heads_here)
        )
        conv_input, input_kept = conv_step(
            convolution_input_cache[layer_number],
            gate_input[:, :, 1],
            input_tap_weight[layer_number],
            lengths,
        )
        maps_f, maps_kept = conv_step(
            convolution_map_cache[layer_number], map_input, map_tap_weight[layer_number], lengths
        )
        gathered = lax.all_gather(maps_f.astype(jnp.bfloat16), "tp", axis=3, tiled=True)
        strided = gathered.reshape(local_sequences, fresh_tokens, 2, N, G)
        group_maps = lax.dynamic_slice_in_dim(strided, group_index, 1, 4)[..., 0].astype(
            jnp.float32
        )
        write_map = jnp.broadcast_to(
            group_maps[:, :, 0][:, :, None, :], (local_sequences, fresh_tokens, heads_here, N)
        )
        read_map = jnp.broadcast_to(
            group_maps[:, :, 1][:, :, None, :], (local_sequences, fresh_tokens, heads_here, N)
        )
        head_step_size = (
            jax.nn.softplus(step_raw.astype(jnp.float32) + step_size_bias[layer_number])
            * active_mask[..., None]
        )
        decay_logarithm = (
            head_step_size * -jnp.exp(decay_rate_logarithm[layer_number])
            + extra_log_decay[layer_number] * active_mask[..., None]
        )
        head_input = conv_input.reshape(local_sequences, fresh_tokens, heads_here, head_size)
        head_gate = (
            gate_input[:, :, 0]
            .astype(jnp.float32)
            .reshape(local_sequences, fresh_tokens, heads_here, head_size)
        )
        mixed_out, state_new = ssd_block(
            head_input,
            head_gate,
            head_step_size,
            decay_logarithm,
            write_map,
            read_map,
            recurrent_state[layer_number],
            direct_path_weight[layer_number],
            head_norm_scale[layer_number].reshape(heads_here, head_size),
        )
        head_out = (
            (mixed_out * active_mask[:, :, None, None])
            .astype(jnp.bfloat16)
            .reshape(own_rows, heads_here * head_size)
        )
        all_heads = lax.all_gather(head_out, "dp", axis=0, tiled=True)
        token_block = lax.all_to_all(all_heads, "tp", split_axis=0, concat_axis=1, tiled=True)
        slice_rows = token_block.shape[0]
        out_block = jnp.dot(
            token_block,
            lax.all_gather(output_weight[layer_number], "tp", axis=0, tiled=True),
            preferred_element_type=jnp.float32,
        )
        residual = lax.dynamic_slice_in_dim(stream_f, head_rank * slice_rows, slice_rows, 0)
        stream = lax.all_gather(residual + out_block, "tp", axis=0, tiled=True)
        input_states.append(input_kept)
        map_states.append(maps_kept)
        ssm_states.append(state_new)
    return (stream, jnp.stack(input_states), jnp.stack(map_states), jnp.stack(ssm_states))


def solution(mesh):
    placed = (
        P(None, "dp"),
        P("dp"),
        P(None, "dp"),
        P(None, "dp", None, "tp"),
        P(None, "dp", None, "tp"),
        P(None, "dp", "tp"),
        P(None, None, "tp"),
        P(None, None, None, "tp"),
        P(None, "tp"),
        P(None, "tp"),
        P(None, "tp"),
        P(None, "tp"),
        P(None, "tp", "dp"),
        P(None, "dp", None, "tp"),
        P(None, "dp", None, None, "tp"),
        P(None, "dp", "tp", None, None),
        P(None, "dp", None, "tp"),
    )
    return jax.shard_map(
        body,
        mesh=mesh,
        in_specs=placed,
        out_specs=(
            P(None, "dp"),
            P(None, "dp", None, "tp"),
            P(None, "dp", None, None, "tp"),
            P(None, "dp", "tp", None, None),
        ),
        check_vma=False,
    )
```

profile of v0, /device:TPU:0, one launch (start us, length us, event | category | flops | bytes accessed | tf_op | source)
XLA Modules:
  0.0 251.9 jit_solution(17837993268887511905)
XLA Ops:
  8.1 0.8 fusion.91
  8.8 1.0 convolution_convert_fusion.9
  9.9 0.7 copy.176
  10.7 1.8 convolution_convert_fusion.3
  12.7 1.9 fusion.87
  14.6 0.9 convolution_convert_fusion.1
  15.6 0.8 fusion.88
  16.5 0.1 multiply_reduce_fusion.1
  16.6 11.4 %psum.14 = f32[128]{0:T(128)S(1)} all-reduce(f32[128]{0:T(128)S(1)} %multiply_reduce_fusion.1), channel_id=1, replica_groups=mesh['tp'=8,'dp'=4] {'dp'}, use_global_device_ids=true, to_apply=%region_2.3 | all-reduce | flops 128 | bytes 1024 | tf_op jit(solution)/shard_map/psum | solution.py:119
  28.5 9.8 %reduce-scatter.19.cloned.1.call-done = bf16[32,4]{1,0:T(8,128)(2,1)} async-done(((bf16[128,4]{1,0:T(8,128)(2,1)}), bf16[32,4]{1,0:T(8,128)(2,1)}) %reduce-scatter.19.cloned.1.call-update) | async-done | bytes 272
  38.4 0.8 copy.177
  39.6 25.6 %reduce-scatter.13.cloned.1.call-done = bf16[32,2,64]{2,0,1:T(8,128)(2,1)} async-done(((bf16[128,2,64]{2,0,1:T(8,128)(2,1)}), bf16[32,2,64]{2,0,1:T(8,128)(2,1)}) %reduce-scatter.13.cloned.1.call-update) | async-done | bytes 8208 | tf_op jit(solution)/shard_map/reduce_scatter | solution.py:126
  65.2 0.8 multiply_convert_fusion.12
  66.0 0.1 copy.130
  66.2 14.7 %all_gather.24 = bf16[2,16,2,512]{1,2,0,3:T(2,128)(2,1)S(1)} all-gather(bf16[2,16,2,64]{1,2,0,3:T(2,128)(2,1)S(1)} %copy.130), channel_id=1, replica_groups=mesh['tp'=8,'dp'=4] {'tp'}, dimensions={3}, use_global_device_ids=true | all-gather | bytes 73728 | tf_op jit(solution)/shard_map/all_gather | solution.py:157
  81.1 0.2 fusion.13
  81.3 0.5 fusion.14
  81.8 10.3 %reduce-scatter.11.cloned.1.call-done = bf16[32,2,256]{2,0,1:T(8,128)(2,1)} async-done(((bf16[128,2,256]{2,0,1:T(8,128)(2,1)}), bf16[32,2,256]{2,0,1:T(8,128)(2,1)}) %reduce-scatter.11.cloned.1.call-update) | async-done | bytes 32784 | tf_op jit(solution)/shard_map/reduce_scatter | solution.py:123
  92.1 0.8 multiply_convert_fusion.8
  93.0 0.1 reshape.250
  93.2 0.1 broadcast_multiply_fusion.1
  93.4 0.4 multiply_reduce_fusion.3
  93.9 0.1 reshape.234
  94.0 8.8 %all_gather.25 = bf16[128,256]{1,0:T(8,128)(2,1)} all-gather(bf16[32,256]{1,0:T(8,128)(2,1)S(1)} %reshape.234), channel_id=1, replica_groups=mesh['tp'=8,'dp'=4] {'dp'}, dimensions={0}, use_global_device_ids=true | all-gather | bytes 81920 | tf_op jit(solution)/shard_map/all_gather | solution.py:198
  102.8 4.6 %all-to-all-start = ((bf16[8,16,256]{2,1,0:T(8,128)(2,1)}), bf16[8,16,256]{2,1,0:T(8,128)(2,1)S(1)}, u32[]{:S(2)}, u32[]{:S(2)}) async-start(bf16[8,16,256]{2,1,0:T(8,128)(2,1)} %bitcast.32), calls=%async_computation.2 | async-start | bytes 131072 | tf_op jit(solution)/shard_map/all_to_all | solution.py:199
  107.5 5.8 %all-to-all-done = bf16[8,16,256]{2,1,0:T(8,128)(2,1)S(1)} async-done(((bf16[8,16,256]{2,1,0:T(8,128)(2,1)}), bf16[8,16,256]{2,1,0:T(8,128)(2,1)S(1)}, u32[]{:S(2)}, u32[]{:S(2)}) %all-to-all-start) | async-done | bytes 65568 | tf_op jit(solution)/shard_map/all_to_all | solution.py:199
  113.4 2.0 fusion.16
  115.3 14.2 %all_gather.27 = f32[128,512]{1,0:T(8,128)S(1)} all-gather(f32[16,512]{1,0:T(8,128)S(1)} %fusion.16), channel_id=1, replica_groups=mesh['tp'=8,'dp'=4] {'tp'}, dimensions={0}, use_global_device_ids=true | all-gather | bytes 294912 | tf_op jit(solution)/shard_map/all_gather | solution.py:207
  129.6 0.1 multiply_reduce_fusion
  129.7 0.1 convolution_convert_fusion.8
  129.8 0.7 copy.178
  130.6 0.8 convolution_convert_fusion.2
  131.5 0.9 convolution_convert_fusion
  132.5 0.5 all-gather.7.cloned.1.call-update
  133.3 0.2 fusion.24
  133.5 0.2 fusion.22
  133.7 0.6 fusion.5
  134.3 8.9 %psum.15 = f32[128]{0:T(128)S(1)} all-reduce(f32[128]{0:T(128)S(1)} %get-tuple-element.30), channel_id=1, replica_groups=mesh['tp'=8,'dp'=4] {'dp'}, use_global_device_ids=true, to_apply=%region_9.10 | all-reduce | flops 128 | bytes 1024 | tf_op jit(solution)/shard_map/psum | solution.py:119
  143.3 9.0 %reduce-scatter.21.cloned.1.call-done = bf16[32,4]{1,0:T(8,128)(2,1)} async-done(((bf16[128,4]{1,0:T(8,128)(2,1)}), bf16[32,4]{1,0:T(8,128)(2,1)}) %reduce-scatter.21.cloned.1.call-update) | async-done | bytes 272
  152.3 0.8 copy.179
  153.5 25.5 %reduce-scatter.17.cloned.1.call-done = bf16[32,2,64]{2,0,1:T(8,128)(2,1)} async-done(((bf16[128,2,64]{2,0,1:T(8,128)(2,1)}), bf16[32,2,64]{2,0,1:T(8,128)(2,1)}) %reduce-scatter.17.cloned.1.call-update) | async-done | bytes 8208 | tf_op jit(solution)/shard_map/reduce_scatter | solution.py:126
  179.0 0.8 multiply_convert_fusion.10
  179.9 0.1 copy.149
  180.0 14.7 %all_gather.28 = bf16[2,16,2,512]{1,2,0,3:T(2,128)(2,1)S(1)} all-gather(bf16[2,16,2,64]{1,2,0,3:T(2,128)(2,1)S(1)} %copy.149), channel_id=1, replica_groups=mesh['tp'=8,'dp'=4] {'tp'}, dimensions={3}, use_global_device_ids=true | all-gather | bytes 73728 | tf_op jit(solution)/shard_map/all_gather | solution.py:157
  194.9 0.2 fusion.25
  195.1 0.6 copy.166
  195.7 0.2 fusion.9
  196.0 0.5 fusion.15
  196.5 10.0 %reduce-scatter.15.cloned.1.call-done = bf16[32,2,256]{2,0,1:T(8,128)(2,1)} async-done(((bf16[128,2,256]{2,0,1:T(8,128)(2,1)}), bf16[32,2,256]{2,0,1:T(8,128)(2,1)}) %reduce-scatter.15.cloned.1.call-update) | async-done | bytes 32784 | tf_op jit(solution)/shard_map/reduce_scatter | solution.py:123
  206.4 0.8 multiply_convert_fusion.6
  207.5 0.1 broadcast_multiply_fusion
  207.7 0.4 multiply_reduce_fusion.2
  208.0 0.1 multiply_convert_fusion.5
  208.2 0.1 reshape.239
  208.3 8.8 %all_gather.29 = bf16[128,256]{1,0:T(8,128)(2,1)} all-gather(bf16[32,256]{1,0:T(8,128)(2,1)S(1)} %reshape.239), channel_id=1, replica_groups=mesh['tp'=8,'dp'=4] {'dp'}, dimensions={0}, use_global_device_ids=true | all-gather | bytes 81920 | tf_op jit(solution)/shard_map/all_gather | solution.py:198
  217.1 4.6 %all-to-all-start.1 = ((bf16[8,16,256]{2,1,0:T(8,128)(2,1)}), bf16[8,16,256]{2,1,0:T(8,128)(2,1)S(1)}, u32[]{:S(2)}, u32[]{:S(2)}) async-start(bf16[8,16,256]{2,1,0:T(8,128)(2,1)} %bitcast.67), calls=%async_computation.5 | async-start | bytes 131072 | tf_op jit(solution)/shard_map/all_to_all | solution.py:199
  221.7 0.2 fusion.23
  221.9 0.6 copy.165
  222.5 0.6 fusion.4
  223.1 0.8 pad_maximum_fusion
  224.0 3.6 %all-to-all-done.1 = bf16[8,16,256]{2,1,0:T(8,128)(2,1)S(1)} async-done(((bf16[8,16,256]{2,1,0:T(8,128)(2,1)}), bf16[8,16,256]{2,1,0:T(8,128)(2,1)S(1)}, u32[]{:S(2)}, u32[]{:S(2)}) %all-to-all-start.1) | async-done | bytes 65568 | tf_op jit(solution)/shard_map/all_to_all | solution.py:199
  227.6 2.0 fusion.19
  229.6 14.2 %all_gather.31 = f32[128,512]{1,0:T(8,128)S(1)} all-gather(f32[16,512]{1,0:T(8,128)S(1)} %fusion.19), channel_id=1, replica_groups=mesh['tp'=8,'dp'=4] {'tp'}, dimensions={0}, use_global_device_ids=true | all-gather | bytes 294912 | tf_op jit(solution)/shard_map/all_gather | solution.py:207
  243.8 0.7 copy.229
  (117 shorter events, 3.1 us)
Async XLA Ops:
  8.0 6.6 %copy-start.1 = (bf16[128,512]{1,0:T(8,128)(2,1)S(1)}, bf16[128,512]{1,0:T(8,128)(2,1)}, u32[]{:S(2)}) copy-start(bf16[128,512]{1,0:T(8,128)(2,1)} %param.17) | copy-start | bytes 393220
  8.0 7.6 %copy-start.2 = (bf16[2,256,512]{2,1,0:T(8,128)(2,1)S(1)}, bf16[2,256,512]{2,1,0:T(8,128)(2,1)}, u32[]{:S(2)}) copy-start(bf16[2,256,512]{2,1,0:T(8,128)(2,1)} %param.29) | copy-start | bytes 1572868
  8.0 30.4 %reduce-scatter.19.cloned.1.call-start = ((), (), s32[]{:S(2)}) async-start(), calls=%async_computation.14 | async-start | bytes 40960
  10.6 54.6 %reduce-scatter.13.cloned.1.call-start = ((), (), s32[]{:S(2)}) async-start(), calls=%async_computation.9 | async-start | bytes 81920 | tf_op jit(solution)/shard_map/reduce_scatter | solution.py:126
  12.5 15.5 %copy-start.6 = (bf16[2,2,3,256]{3,1,2,0:T(2,128)(2,1)S(1)}, bf16[2,2,3,256]{3,1,2,0:T(2,128)(2,1)}, u32[]{:S(2)}) copy-start(bf16[2,2,3,256]{3,1,2,0:T(2,128)(2,1)} %param.30) | copy-start | bytes 18436
  12.5 15.5 %copy-start.4 = (bf16[2,4,256]{2,1,0:T(4,128)(2,1)S(1)}, bf16[2,4,256]{2,1,0:T(4,128)(2,1)}, u32[]{:S(2)}) copy-start(bf16[2,4,256]{2,1,0:T(4,128)(2,1)} %param.23) | copy-start | bytes 12292
  12.5 15.5 %copy-start.11 = (f32[2,4]{1,0:T(2,128)S(1)}, f32[2,4]{1,0:T(2,128)}, u32[]{:S(2)}) copy-start(f32[2,4]{1,0:T(2,128)} %param.27) | copy-start | bytes 100
  12.5 15.5 %copy-start.5 = (f32[2,2,16,4]{2,3,1,0:T(4,128)S(1)}, f32[2,2,16,4]{2,3,1,0:T(4,128)}, u32[]{:S(2)}) copy-start(f32[2,2,16,4]{2,3,1,0:T(4,128)} %param.33) | copy-start | bytes 3076
  12.6 15.6 %copy-start.14 = (s32[2]{0:T(128)S(1)}, s32[2]{0:T(128)}, u32[]{:S(2)}) copy-start(s32[2]{0:T(128)} %param.18) | copy-start | bytes 28
  12.6 15.7 %copy-start.7 = (bf16[2,2,3,2,64]{4,3,2,1,0:T(2,128)(2,1)S(1)}, bf16[2,2,3,2,64]{4,3,2,1,0:T(2,128)(2,1)}, u32[]{:S(2)}) copy-start(bf16[2,2,3,2,64]{4,3,2,1,0:T(2,128)(2,1)} %param.31) | copy-start | bytes 9220
  12.6 15.7 %copy-start.8 = (bf16[2,4,2,64]{3,2,1,0:T(2,128)(2,1)S(1)}, bf16[2,4,2,64]{3,2,1,0:T(2,128)(2,1)}, u32[]{:S(2)}) copy-start(bf16[2,4,2,64]{3,2,1,0:T(2,128)(2,1)} %param.24) | copy-start | bytes 6148
  12.6 15.7 %copy-start.10 = (f32[2,256]{1,0:T(2,128)S(1)}, f32[2,256]{1,0:T(2,128)}, u32[]{:S(2)}) copy-start(f32[2,256]{1,0:T(2,128)} %param.28) | copy-start | bytes 6148
  12.6 15.9 %copy-start.12 = (f32[2,4]{1,0:T(2,128)S(1)}, f32[2,4]{1,0:T(2,128)}, u32[]{:S(2)}) copy-start(f32[2,4]{1,0:T(2,128)} %param.25) | copy-start | bytes 100
  12.6 15.9 %copy-start.13 = (f32[2,4]{1,0:T(2,128)S(1)}, f32[2,4]{1,0:T(2,128)}, u32[]{:S(2)}) copy-start(f32[2,4]{1,0:T(2,128)} %param.26) | copy-start | bytes 100
  12.6 79.5 %reduce-scatter.11.cloned.1.call-start = ((), (), s32[]{:S(2)}) async-start(), calls=%async_computation.8 | async-start | bytes 163840 | tf_op jit(solution)/shard_map/reduce_scatter | solution.py:123
  14.6 66.7 %copy-start = (f32[2,2,4,64,128]{4,3,2,1,0:T(8,128)S(1)}, f32[2,2,4,64,128]{4,3,2,1,0:T(8,128)}, u32[]{:S(2)}) copy-start(f32[2,2,4,64,128]{4,3,2,1,0:T(8,128)} %param.32) | copy-start | bytes 1572868
  15.5 97.8 %all-gather.5.cloned.1.call-start = ((), (), s32[]{:S(2)}) async-start(), calls=%async_computation.12 | async-start | bytes 2359296 | tf_op jit(solution)/shard_map/all_gather | solution.py:203
  93.4 36.3 %copy-start.9 = (bf16[2,512,4]{1,2,0:T(4,128)(2,1)S(1)}, bf16[2,512,4]{1,2,0:T(4,128)(2,1)}, u32[]{:S(2)}) copy-start(bf16[2,512,4]{1,2,0:T(4,128)(2,1)} %param.22) | copy-start | bytes 24580
  93.8 36.9 %copy-start.3 = (bf16[2,512,2,64]{1,3,2,0:T(8,128)(2,1)S(1)}, bf16[2,512,2,64]{1,3,2,0:T(8,128)(2,1)}, u32[]{:S(2)}) copy-start(bf16[2,512,2,64]{1,3,2,0:T(8,128)(2,1)} %param.21) | copy-start | bytes 786436
  102.8 10.5 %all-to-all-start = ((bf16[8,16,256]{2,1,0:T(8,128)(2,1)}), bf16[8,16,256]{2,1,0:T(8,128)(2,1)S(1)}, u32[]{:S(2)}, u32[]{:S(2)}) async-start(bf16[8,16,256]{2,1,0:T(8,128)(2,1)} %bitcast.32), calls=%async_computation.2 | async-start | bytes 131072 | tf_op jit(solution)/shard_map/all_to_all | solution.py:199
  107.4 44.9 %reduce-scatter.21.cloned.1.call-start = ((), (), s32[]{:S(2)}) async-start(), calls=%async_computation.15 | async-start | bytes 40960
  130.6 48.5 %reduce-scatter.17.cloned.1.call-start = ((), (), s32[]{:S(2)}) async-start(), calls=%async_computation.11 | async-start | bytes 81920 | tf_op jit(solution)/shard_map/reduce_scatter | solution.py:126
  131.5 74.9 %reduce-scatter.15.cloned.1.call-start = ((), (), s32[]{:S(2)}) async-start(), calls=%async_computation.10 | async-start | bytes 163840 | tf_op jit(solution)/shard_map/reduce_scatter | solution.py:123
  132.5 95.2 %all-gather.7.cloned.1.call-start = ((), (), s32[]{:S(2)}) async-start(), calls=%async_computation.13 | async-start | bytes 2359296 | tf_op jit(solution)/shard_map/all_gather | solution.py:203
  217.1 10.5 %all-to-all-start.1 = ((bf16[8,16,256]{2,1,0:T(8,128)(2,1)}), bf16[8,16,256]{2,1,0:T(8,128)(2,1)S(1)}, u32[]{:S(2)}, u32[]{:S(2)}) async-start(bf16[8,16,256]{2,1,0:T(8,128)(2,1)} %bitcast.67), calls=%async_computation.5 | async-start | bytes 131072 | tf_op jit(solution)/shard_map/all_to_all | solution.py:199
Sparse Core Ops, SparseCore 0:
  11.5 26.7 reduce-scatter.18
  41.1 24.0 reduce-scatter.12
  67.9 24.1 reduce-scatter.10
  130.7 21.6 reduce-scatter.20
  154.9 24.0 reduce-scatter.16
  182.2 24.1 reduce-scatter.14
Sparse Core Ops, SparseCore 1:
  18.2 31.8 all-gather.4
  135.1 26.6 all-gather.6
where the time goes:
time: 253 us; the launch traced here: 252 us
  waiting for transfers between devices  100 us (40%)
  blocking collectives  95.8 us (38%)
  between operations  16.1 us (6%)
  matrix products  13.7 us (5%)
  local copies, waits for them, and re-layouts  10.8 us (4%)
  starting transfers between devices  9.57 us (4%)
  other arithmetic  5.5 us (2%)
    reduce_scatter x2, waiting for transfers between devices, body(): lax.psum_scatter(maps_partial.astype(jnp.bfloat16), 'dp', scatter_dimensi...  51.1 us
    all_gather x2, blocking collectives, body(): lax.all_gather(maps_f.astype(jnp.bfloat16), 'tp', axis=3, tiled=True)  29.5 us
    all_gather x2, blocking collectives, body(): stream = lax.all_gather(residual + out_block, 'tp', axis=0, tiled=True)  28.5 us
    psum x2, blocking collectives, body(): squares = lax.psum(row_squares, 'dp')  20.3 us
    reduce_scatter x2, waiting for transfers between devices, body(): lax.psum_scatter(pair_partial.astype(jnp.bfloat16), 'dp', scatter_dimensi...  20.3 us
    unnamed x10, waiting for transfers between devices  19.5 us
    all_gather x2, blocking collectives, body(): all_heads = lax.all_gather(head_out, 'dp', axis=0, tiled=True)  17.6 us
    all_to_all x2, waiting for transfers between devices, body(): lax.all_to_all(all_heads, 'tp', split_axis=0, concat_axis=1, tiled=True)  9.49 us
  transfers between devices with their start and end apart: 10, of which 8 were waited for; matrix products, arithmetic and copies ran while one was open for 9% of the time, Pallas kernels for 0%

commit v1 on v0

v1 whole, which is shorter than its diff:
```python
import functools

import jax
import jax.numpy as jnp
import numpy as np
from jax import lax
from jax.experimental import pallas as pl
from jax.experimental.pallas import tpu as pltpu
from jax.sharding import PartitionSpec as P

EPS = 1e-06
LANES = 128
FRONT = 8
HIGHEST = lax.Precision.HIGHEST
F32, BF16 = jnp.float32, jnp.bfloat16


def up(n):
    return -(-n // LANES) * LANES


def dot(a, b, ca=1, cb=0, precision=None):
    return lax.dot_general(
        a, b, (((ca,), (cb,)), ((), ())), precision=precision, preferred_element_type=F32
    )


def kernel(
    n_tp, n_dp, d_model, heads, groups, slots, seqs, hp_cols, map_cols,
    lens, x, scale, w, taps, cache, par, hv, extra, state, wout, sel, sel2, tri, ex, ext, ones,
    stream, kept, ssm,
    a_send, a_recv, m_send, m_recv, h_send, h_recv, o_send, o_recv, n_send, n_recv, padded,
    a_ss, a_rs, m_ss, m_rs, h_ss, h_rs, o_ss, o_rs, n_ss, n_rs,
):
    tp, dp = lax.axis_index("tp"), lax.axis_index("dp")
    layers = w.shape[0]
    rows = seqs * slots
    taps_n = taps.shape[1]
    keep = taps_n - 1
    zc = up(hp_cols)
    ng = map_cols // groups
    n_state = state.shape[-1]
    cut = stream.shape[0] // n_tp
    per = rows // cut
    head_size = hp_cols // heads

    barrier = pltpu.get_barrier_semaphore()
    for k in range(1, n_dp):
        pl.semaphore_signal(barrier, inc=1, device_id={"dp": lax.rem(dp + k, n_dp)})
    for k in range(1, n_tp):
        pl.semaphore_signal(barrier, inc=1, device_id={"tp": lax.rem(tp + k, n_tp)})

    stream[...] = x[...].astype(F32)
    slot = lax.broadcasted_iota(jnp.int32, (slots, 1), 0)
    mask = jnp.concatenate([(slot < lens[s]).astype(F32) for s in range(seqs)], axis=0)
    lane = lax.broadcasted_iota(jnp.int32, (1, LANES), 1)
    r_id = lax.broadcasted_iota(jnp.int32, (rows, rows), 0)
    c_id = lax.broadcasted_iota(jnp.int32, (rows, rows), 1)
    causal = tri[...] > 0.5
    padded[...] = jnp.zeros_like(padded)
    sends = []

    def copy(src, dst, ss, rs, where):
        return pltpu.make_async_remote_copy(
            src_ref=src, dst_ref=dst, send_sem=ss, recv_sem=rs, device_id=where
        )

    for l in range(layers):
        st = stream[...]
        squares = jnp.sum(st * st, axis=1, keepdims=True)
        normed = (st * scale[l : l + 1, :]).astype(BF16)
        part = dot(normed, w[l])
        tail = part[:, part.shape[1] - LANES :]
        high = squares.astype(BF16).astype(F32)
        tail = jnp.where(lane == LANES - 2, high, jnp.where(lane == LANES - 1, squares - high, tail))
        part = jnp.concatenate([part[:, : part.shape[1] - LANES], tail], axis=1).astype(BF16)
        for b in range(n_dp):
            a_send[l, b] = part[b * rows : (b + 1) * rows]
        if l == 0:
            pl.semaphore_wait(barrier, n_dp - 1 + n_tp - 1)
        flights = []
        for k in range(1, n_dp):
            to = lax.rem(dp + k, n_dp)
            c = copy(a_send.at[l, to], a_recv.at[l, k - 1], a_ss.at[l, k - 1], a_rs.at[l, k - 1], {"dp": to})
            c.start()
            flights.append(c)
        sends += flights
        acc = a_send[l, dp].astype(F32)
        for k, c in enumerate(flights):
            c.wait_recv()
            acc = acc + a_recv[l, k].astype(F32)
        tail = acc[:, acc.shape[1] - LANES :]
        squares = tail[:, LANES - 2 : LANES - 1] + tail[:, LANES - 1 : LANES]
        factor = lax.rsqrt(squares / d_model + EPS)
        proj = (acc * factor).astype(BF16).astype(F32)

        conv_w = taps.shape[2]
        pieces = []
        for s in range(seqs):
            padded[s, FRONT - keep : FRONT, :] = cache[l, s].astype(F32)
            padded[s, FRONT : FRONT + slots, :] = proj[s * slots : (s + 1) * slots, zc : zc + conv_w]
            total = padded[s, FRONT - keep : FRONT - keep + slots, :] * taps[l, 0:1, :]
            for t in range(1, taps_n):
                at = FRONT - keep + t
                total = total + padded[s, at : at + slots, :] * taps[l, t : t + 1, :]
            pieces.append(total)
        filtered = jnp.concatenate(pieces, axis=0)
        filtered = filtered * jax.nn.sigmoid(filtered)
        maps = filtered[:, conv_w - up(2 * map_cols) :].astype(BF16)
        sorted_maps = dot(sel[...], maps, 1, 1)
        for g in range(groups):
            m_send[l, g] = sorted_maps[g * 2 * ng : (g + 1) * 2 * ng, :].astype(BF16)

        def group_of(rank):
            return rank * heads // (heads * n_tp // groups)

        flights = []
        for k in range(1, n_tp):
            to = lax.rem(tp + k, n_tp)
            c = copy(m_send.at[l, group_of(to)], m_recv.at[l, tp], m_ss.at[l, k - 1], m_rs.at[l, k - 1], {"tp": to})
            c.start()
            flights.append(c)
        sends += flights
        m_recv[l, tp] = m_send[l, group_of(tp)]

        for s in range(seqs):
            pick = lax.broadcasted_iota(jnp.int32, (8, FRONT + slots), 0)
            place = lax.broadcasted_iota(jnp.int32, (8, FRONT + slots), 1)
            chooser = ((place == pick + lens[s] + (FRONT - keep)) & (pick < keep)).astype(BF16)
            kept[l, s] = dot(chooser, padded[s].astype(BF16)).astype(BF16)
        raw = proj[:, proj.shape[1] - LANES :] + par[l, 0:1, :]
        step = (jnp.maximum(raw, 0.0) + jnp.log1p(jnp.exp(-jnp.abs(raw)))) * mask
        step = jnp.where(lane < heads, step, 0.0)
        logdec = extra[l] * mask - step * jnp.exp(par[l, 1:2, :])
        logdec = jnp.where(lane < heads, logdec, 0.0)
        sums = dot(tri[...], logdec, precision=HIGHEST)
        sums_t = sums.T
        step_t = step.T
        both = dot(jnp.concatenate([sums, step], axis=0), ex[...], precision=HIGHEST)
        sums_x, step_x = both[:rows], both[rows:]
        inp = filtered[:, :hp_cols]
        gate = proj[:, :hp_cols]
        last_x = jnp.concatenate(
            [
                jnp.broadcast_to(sums_x[(s + 1) * slots - 1 : (s + 1) * slots, :], (slots, hp_cols))
                for s in range(seqs)
            ],
            axis=0,
        )
        weighted = (jnp.exp(last_x - sums_x) * step_x * inp).astype(BF16)
        inp_b = inp.astype(BF16)
        grow = jnp.exp(sums_x)
        direct = hv[l, 0:1, :] * inp
        gate = gate * jax.nn.sigmoid(gate)
        rows_sum = dot(ext[...], sums, 1, 1, precision=HIGHEST)
        segs = []
        for h in range(heads):
            gap = sums[:, h : h + 1] - sums_t[h : h + 1, :]
            segs.append(jnp.exp(jnp.where(causal, gap, -jnp.inf)) * step_t[h : h + 1, :])

        for c in flights:
            c.wait_recv()
        got = m_recv[l].astype(F32).reshape(n_tp * 2 * ng, rows)
        both_maps = dot(got.T.astype(BF16), sel2[...]).astype(BF16)
        b_map, c_map = both_maps[:, :n_state], both_maps[:, n_state:]
        cross = dot(c_map, b_map, 1, 1)
        within = jnp.concatenate(
            [
                dot((cross * segs[h]).astype(BF16), inp_b[:, h * head_size : (h + 1) * head_size])
                for h in range(heads)
            ],
            axis=1,
        )
        carried = jnp.concatenate(
            [
                dot(c_map[s * slots : (s + 1) * slots], state[l, s].astype(BF16), 1, 1)
                for s in range(seqs)
            ],
            axis=0,
        )
        read = (within + carried * grow + direct) * gate
        power = read * read
        p_hi = power.astype(BF16)
        p_lo = (power - p_hi.astype(F32)).astype(BF16)
        mean = (dot(p_hi, ones[...]) + dot(p_lo, ones[...])) / head_size
        headout = (read * lax.rsqrt(mean + EPS) * hv[l, 1:2, :] * mask).astype(BF16)
        h_send[l] = headout
        flights = []
        for k in range(1, n_dp):
            to = lax.rem(dp + k, n_dp)
            c = copy(h_send.at[l], h_recv.at[l, k - 1], h_ss.at[l, k - 1], h_rs.at[l, k - 1], {"dp": to})
            c.start()
            flights.append(c)
        sends += flights

        def push(value, block):
            out = dot(value, wout[l]).astype(BF16)
            for i in range(per):
                to = block * per + i
                o_send[l, to] = out[i * cut : (i + 1) * cut]

                @pl.when(to != tp)
                def _():
                    copy(o_send.at[l, to], o_recv.at[l, tp], o_ss.at[l, to], o_rs.at[l, tp], {"tp": to}).start()

        push(headout, dp)
        for s in range(seqs):
            at = slice(s * slots, (s + 1) * slots)
            fresh = dot(weighted[at], b_map[at], 0, 0)
            end = (s + 1) * slots - 1
            ssm[l, s] = jnp.exp(rows_sum[:, end : end + 1]) * state[l, s] + fresh
        for k, c in enumerate(flights):
            c.wait_recv()
            push(h_recv[l, k], lax.rem(dp + n_dp - k - 1, n_dp))
        total = o_send[l, tp].astype(F32)
        for k in range(1, n_tp):
            src = lax.rem(tp + n_tp - k, n_tp)
            copy(o_send.at[l, src], o_recv.at[l, src], o_ss.at[l, src], o_rs.at[l, src], {"tp": src}).wait_recv()
            total = total + o_recv[l, src].astype(F32)
        fresh = total.astype(BF16)
        n_send[l] = fresh
        n_recv[l, tp] = fresh
        flights = []
        for k in range(1, n_tp):
            to = lax.rem(tp + k, n_tp)
            c = copy(n_send.at[l], n_recv.at[l, tp], n_ss.at[l, k - 1], n_rs.at[l, k - 1], {"tp": to})
            c.start()
            flights.append(c)
        sends += flights
        for c in flights:
            c.wait_recv()
        stream[...] += n_recv[l].astype(F32).reshape(stream.shape)

    for c in sends:
        c.wait_send()
    for l in range(layers):
        for k in range(1, n_tp):
            to = lax.rem(tp + k, n_tp)
            copy(o_send.at[l, to], o_recv.at[l, tp], o_ss.at[l, to], o_rs.at[l, tp], {"tp": to}).wait_send()


def body(
    n_tp, n_dp,
    tokens, lengths, input_norm_scale, gate_input_weight, maps_weight, step_weight,
    input_tap_weight, map_tap_weight, step_size_bias, decay_rate_logarithm, direct_path_weight,
    head_norm_scale, output_weight, convolution_input_cache, convolution_map_cache,
    recurrent_state, extra_log_decay,
):
    layers, seqs, slots, heads = extra_log_decay.shape
    head_size, n_state = recurrent_state.shape[3:]
    hp_cols = heads * head_size
    map_cols = maps_weight.shape[3]
    groups = map_cols * n_tp // n_state
    ng = map_cols // groups
    rows = seqs * slots
    d_here = tokens.shape[1]
    keep = convolution_input_cache.shape[2]

    def wide(a):
        pad = up(a.shape[-1]) - a.shape[-1]
        return a if pad == 0 else jnp.pad(a, [(0, 0)] * (a.ndim - 1) + [(0, pad)])

    w = jnp.concatenate(
        [
            wide(gate_input_weight[:, :, 0]),
            wide(gate_input_weight[:, :, 1]),
            wide(maps_weight.reshape(layers, d_here, 2 * map_cols)),
            wide(step_weight),
        ],
        axis=2,
    )
    taps = jnp.concatenate(
        [wide(input_tap_weight), wide(map_tap_weight.reshape(layers, -1, 2 * map_cols))], axis=2
    ).astype(F32)
    cache = jnp.concatenate(
        [
            wide(convolution_input_cache),
            wide(convolution_map_cache.reshape(layers, seqs, keep, 2 * map_cols)),
        ],
        axis=3,
    )
    par = wide(jnp.stack([step_size_bias, decay_rate_logarithm], axis=1))
    hv = jnp.stack([jnp.repeat(direct_path_weight, head_size, axis=1), head_norm_scale], axis=1)
    extra = wide(extra_log_decay.reshape(layers, rows, heads))
    state = recurrent_state.reshape(layers, seqs, hp_cols, n_state)

    sel = np.zeros((2 * map_cols, up(2 * map_cols)), np.float32)
    for g in range(groups):
        for which in range(2):
            for j in range(ng):
                sel[g * 2 * ng + which * ng + j, which * map_cols + groups * j + g] = 1
    sel2 = np.zeros((n_tp * 2 * ng, 2 * n_state), np.float32)
    for src in range(n_tp):
        for which in range(2):
            for j in range(ng):
                sel2[src * 2 * ng + which * ng + j, which * n_state + src * ng + j] = 1
    tri = np.kron(np.eye(seqs), np.tril(np.ones((slots, slots)))).astype(np.float32)
    ex = np.zeros((LANES, hp_cols), np.float32)
    ex[:heads] = np.kron(np.eye(heads), np.ones((1, head_size)))
    ones = np.kron(np.eye(heads), np.ones((head_size, head_size))).astype(np.float32)

    vmem = pl.BlockSpec(memory_space=pltpu.VMEM)
    wide_cols = w.shape[2]
    conv_w = taps.shape[2]
    cut = tokens.shape[0] // n_tp
    sems = lambda n: pltpu.SemaphoreType.DMA((layers, n))
    args = [
        tokens, input_norm_scale, w, taps, cache, par, hv, extra, state, output_weight,
        jnp.asarray(sel, BF16), jnp.asarray(sel2, BF16), jnp.asarray(tri), jnp.asarray(ex),
        jnp.asarray(ex.T.copy()), jnp.asarray(ones, BF16),
    ]
    stream, kept, ssm = pl.pallas_call(
        functools.partial(
            kernel, n_tp, n_dp, d_here * n_dp, heads, groups, slots, seqs, hp_cols, map_cols
        ),
        out_shape=(
            jax.ShapeDtypeStruct(tokens.shape, F32),
            jax.ShapeDtypeStruct((layers, seqs, 8, conv_w), BF16),
            jax.ShapeDtypeStruct(state.shape, F32),
        ),
        in_specs=[pl.BlockSpec(memory_space=pltpu.SMEM)] + [vmem] * len(args),
        out_specs=(vmem, vmem, vmem),
        scratch_shapes=[
            pltpu.VMEM((layers, n_dp, rows, wide_cols), BF16),
            pltpu.VMEM((layers, n_dp - 1, rows, wide_cols), BF16),
            pltpu.VMEM((layers, groups, 2 * ng, rows), BF16),
            pltpu.VMEM((layers, n_tp, 2 * ng, rows), BF16),
            pltpu.VMEM((layers, rows, hp_cols), BF16),
            pltpu.VMEM((layers, n_dp - 1, rows, hp_cols), BF16),
            pltpu.VMEM((layers, n_tp, cut, d_here), BF16),
            pltpu.VMEM((layers, n_tp, cut, d_here), BF16),
            pltpu.VMEM((layers, cut, d_here), BF16),
            pltpu.VMEM((layers, n_tp, cut, d_here), BF16),
            pltpu.VMEM((seqs, FRONT + slots, conv_w), F32),
            sems(n_dp - 1), sems(n_dp - 1), sems(n_tp - 1), sems(n_tp - 1), sems(n_dp - 1),
            sems(n_dp - 1), sems(n_tp), sems(n_tp), sems(n_tp - 1), sems(n_tp - 1),
        ],
        compiler_params=pltpu.CompilerParams(
            collective_id=0, has_side_effects=True, vmem_limit_bytes=48 * 2**20
        ),
        name="mixer",
    )(lengths, *args)
    conv_in = kept[:, :, :keep, :hp_cols]
    start = conv_w - up(2 * map_cols)
    conv_maps = kept[:, :, :keep, start : start + 2 * map_cols].reshape(
        layers, seqs, keep, 2, map_cols
    )
    return stream, conv_in, conv_maps, ssm.reshape(recurrent_state.shape)


def solution(mesh):
    placed = (
        P(None, "dp"),
        P("dp"),
        P(None, "dp"),
        P(None, "dp", None, "tp"),
        P(None, "dp", None, "tp"),
        P(None, "dp", "tp"),
        P(None, None, "tp"),
        P(None, None, None, "tp"),
        P(None, "tp"),
        P(None, "tp"),
        P(None, "tp"),
        P(None, "tp"),
        P(None, "tp", "dp"),
        P(None, "dp", None, "tp"),
        P(None, "dp", None, None, "tp"),
        P(None, "dp", "tp", None, None),
        P(None, "dp", None, "tp"),
    )
    return jax.shard_map(
        functools.partial(body, mesh.shape["tp"], mesh.shape["dp"]),
        mesh=mesh,
        in_specs=placed,
        out_specs=(
            P(None, "dp"),
            P(None, "dp", None, "tp"),
            P(None, "dp", None, None, "tp"),
            P(None, "dp", "tp", None, None),
        ),
        check_vma=False,
    )
```

time: 253 us -> 65.3 us (0.26)
  waiting for transfers between devices: 100 us -> 0 us
  blocking collectives: 95.8 us -> 0 us
  Pallas kernels: 0 us -> 49.5 us
  between operations: 16.1 us -> 0.92 us
  matrix products: 13.7 us -> 0 us
  starting transfers between devices: 9.57 us -> 0 us
  other arithmetic: 5.5 us -> 1.41 us
    all_gather x6 -> x0, blocking collectives: 75.5 us -> none  [the longest x2 29.5 us: body(): lax.all_gather(maps_f.astype(jnp.bfloat16), 'tp', axis=3, tiled=True)]
    reduce_scatter x4 -> x0, waiting for transfers between devices: 71.4 us -> none  [the longest x2 51.1 us: body(): lax.psum_scatter(maps_partial.astype(jnp.bfloat16), 'dp', scatter_dimensi...]
    pallas_call x0 -> x1, Pallas kernels: none -> 49.5 us  [body(): pl.pallas_call(functools.partial(kernel, n_tp, n_dp, d_here * n_dp, heads...]
    psum x2 -> x0, blocking collectives: 20.3 us -> none  [body(): squares = lax.psum(row_squares, 'dp')]
    unnamed x10 -> x0, waiting for transfers between devices: 19.5 us -> none
    dot_general x20 -> x0, matrix products: 13.7 us -> none  [the longest x2 3.94 us: body(): jnp.dot(token_block, lax.all_gather(output_weight[layer_number], 'tp', ax...]
    all_to_all x2 -> x0, waiting for transfers between devices: 9.49 us -> none  [body(): lax.all_to_all(all_heads, 'tp', split_axis=0, concat_axis=1, tiled=True)]
    all_to_all x2 -> x0, starting transfers between devices: 9.24 us -> none  [body(): lax.all_to_all(all_heads, 'tp', split_axis=0, concat_axis=1, tiled=True)]
  transfers between devices with their start and end apart: 10 -> 0, of which waited for: 8 -> 0; matrix products, arithmetic and copies ran while one was open for 9% -> 0% of each run, Pallas kernels for 0% -> 0%
where the time goes in v1:
time: 65.3 us; the launch traced here: 65 us
  Pallas kernels  49.5 us (76%)
  local copies, waits for them, and re-layouts  13.2 us (20%)
  other arithmetic  1.41 us (2%)
  between operations  0.92 us (1%)
    pallas_call x1, Pallas kernels, body(): pl.pallas_call(functools.partial(kernel, n_tp, n_dp, d_here * n_dp, heads...  49.5 us
    unnamed x50, local copies, waits for them, and re-layouts  7.01 us
    slice x1, local copies, waits for them, and re-layouts, body(): gate_input_weight[:, :, 0]  3.27 us
    concatenate x1, other arithmetic, body(): jnp.concatenate([wide(gate_input_weight[:, :, 0]), wide(gate_input_weight...  1.38 us

profile of v1, /device:TPU:0, one launch (start us, length us, event | category | flops | bytes accessed | tf_op | source)
XLA Modules:
  0.0 65.0 jit_solution(14451740952987084847)
XLA Ops:
  0.6 3.3 %fusion.2 = (bf16[2,512,1,256]{3,2,1,0:T(2,128)(2,1)S(1)}, bf16[2,512,1,256]{3,2,1,0:T(2,128)(2,1)S(1)}) fusion(bf16[2,512,2,256]{3,2,1,0:T(2,128)(2,1)} %param.26), kind=kLoop, calls=%fused_computation.9 | loop fusion | bytes 2097152 | tf_op jit(solution)/shard_map/slice | solution.py:265
  3.9 0.0 copy-start.12
  3.9 0.0 copy-start.11
  3.9 1.0 %copy_bitcast_fusion = (bf16[2,512,256]{2,1,0:T(8,128)(2,1)S(1)}, bf16[2,512,256]{2,1,0:T(8,128)(2,1)}) fusion(bf16[2,512,1,256]{3,2,1,0:T(2,128)(2,1)S(1)} %get-tuple-element.19, bf16[2,512,1,256]{3,2,1,0:T(2,128)(2,1)S(1)} %get-tuple-element.18), kind=kLoop, calls=%fused_computation.3 | loop fusion | bytes 2097152 | tf_op jit(solution)/shard_map/squeeze | solution.py:266
  4.9 0.0 copy-done.12
  4.9 0.2 copy.38
  5.1 0.0 copy-done.11
  5.2 0.8 %copy.39 = bf16[2,512,128]{2,1,0:T(8,128)(2,1)} copy(bf16[2,512,128]{1,2,0:T(8,128)(2,1)S(1)} %bitcast.16) | data formatting | bytes 524288 | tf_op jit(solution)/shard_map/reshape | solution.py:267
  6.0 0.0 copy-start.13
  6.0 0.0 copy-start.14
  6.0 0.0 copy-start.15
  6.0 0.0 copy-start.16
  6.0 0.0 copy-start.17
  6.0 0.0 copy-start.19
  6.0 0.0 copy-start.18
  6.0 0.0 copy-start.20
  6.1 0.0 copy-start.21
  6.1 0.0 copy-start
  6.1 0.0 copy-start.1
  6.1 0.0 copy-start.7
  6.1 0.0 copy-start.8
  6.1 0.0 copy-start.9
  6.1 0.0 copy-start.10
  6.1 1.4 %fusion.1.w = bf16[2,512,768]{2,1,0:T(8,128)(2,1)S(1)} fusion(bf16[2,512,4]{2,1,0:T(8,128)(2,1)S(1)} %copy.38, bf16[2,512,128]{2,1,0:T(8,128)(2,1)} %copy.39, bf16[2,512,256]{2,1,0:T(8,128)(2,1)S(1)} %get-tuple-element.20, bf16[2,512,256]{2,1,0:T(8,128)(2,1)} %get-tuple-element.21), kind=kLoop, calls=%fused_computation.2 | loop fusion | flops 7864320 | bytes 2891776 | tf_op jit(solution)/shard_map/concatenate | solution.py:263
  7.5 0.0 copy-done.13
  7.5 0.1 copy.45
  7.6 0.0 copy-done.14
  7.7 0.0 copy-done.15
  7.7 0.1 reshape.36
  7.8 0.0 copy-done.16
  7.8 0.1 reshape.30
  7.9 0.0 copy-done.17
  7.9 0.0 copy-done.19
  7.9 0.1 broadcast_in_dim.3
  8.0 0.1 stack_reshape.3
  8.0 0.0 copy-done.18
  8.1 0.0 copy-done.20
  8.1 0.0 copy-done.21
  8.1 0.0 copy-done
  8.1 0.0 copy-done.1
  8.1 0.0 copy-done.7
  8.1 0.0 copy-done.8
  8.1 0.0 copy-done.9
  8.1 0.0 copy-done.10
  8.2 0.0 copy-start.2
  8.2 0.9 %copy-done.2 = bf16[128,512]{1,0:T(8,128)(2,1)S(1)} copy-done((bf16[128,512]{1,0:T(8,128)(2,1)S(1)}, bf16[128,512]{1,0:T(8,128)(2,1)}, u32[]{:S(2)}) %copy-start.2) | copy-done | bytes 131096
  9.1 0.0 copy-start.3
  9.1 0.9 %copy-done.3 = bf16[256,256]{1,0:T(8,128)(2,1)S(1)} copy-done((bf16[256,256]{1,0:T(8,128)(2,1)S(1)}, bf16[256,256]{1,0:T(8,128)(2,1)}, u32[]{:S(2)}) %copy-start.3) | copy-done | bytes 131096
  10.0 0.0 copy-start.4
  10.0 0.9 %copy-done.4 = f32[128,256]{1,0:T(8,128)S(1)} copy-done((f32[128,256]{1,0:T(8,128)S(1)}, f32[128,256]{1,0:T(8,128)}, u32[]{:S(2)}) %copy-start.4) | copy-done | bytes 131096
  10.9 0.0 copy-start.5
  10.9 0.9 %copy-done.5 = f32[256,128]{1,0:T(8,128)S(1)} copy-done((f32[256,128]{1,0:T(8,128)S(1)}, f32[256,128]{1,0:T(8,128)}, u32[]{:S(2)}) %copy-start.5) | copy-done | bytes 131096
  11.8 0.0 copy-start.6
  11.8 0.9 %copy-done.6 = bf16[256,256]{1,0:T(8,128)(2,1)S(1)} copy-done((bf16[256,256]{1,0:T(8,128)(2,1)S(1)}, bf16[256,256]{1,0:T(8,128)(2,1)}, u32[]{:S(2)}) %copy-start.6) | copy-done | bytes 131096
  12.7 49.5 %mixer.1 = (f32[128,512]{1,0:T(8,128)S(1)}, bf16[2,2,8,384]{3,2,1,0:T(8,128)(2,1)S(1)}, f32[2,2,256,128]{3,2,1,0:T(8,128)S(1)}) custom-call(s32[2]{0:T(128)S(1)} %copy-done.10, bf16[128,512]{1,0:T(8,128)(2,1)S(1)} %copy-done.2, f32[2,512]{1,0:T(2,128)S(1)} %copy-done.9, bf16[2,512,768]{2,1,0:T(8,128)(2,1)S(1)} %fusion.1.w, ...), custom_call_target="tpu_custom_call" | custom-call | tf_op jit(solution)/shard_map/mixer/pallas_call | solution.py:312
  62.2 0.6 copy.47
  62.8 0.7 %reshape.37 = bf16[2,2,3,2,64]{4,3,2,1,0:T(2,128)(2,1)} reshape(bf16[2,2,3,128]{3,2,1,0:T(4,128)(2,1)S(1)} %slice.15) | data formatting | bytes 6144 | tf_op jit(solution)/shard_map/reshape | solution.py:345
  63.5 0.7 %copy.57 = f32[128,512]{1,0:T(8,128)} copy(f32[128,512]{1,0:T(8,128)S(1)} %get-tuple-element.26) | data formatting | bytes 524288
  64.2 0.8 %copy.58 = f32[2,2,4,64,128]{4,3,2,1,0:T(8,128)} copy(f32[2,2,4,64,128]{4,3,2,1,0:T(8,128)S(1)} %bitcast.15) | data formatting | bytes 1048576
  (9 shorter events, 0.1 us)
Async XLA Ops:
  3.9 1.0 %copy-start.12 = (bf16[2,512,4]{1,2,0:T(4,128)(2,1)S(1)}, bf16[2,512,4]{1,2,0:T(4,128)(2,1)}, u32[]{:S(2)}) copy-start(bf16[2,512,4]{1,2,0:T(4,128)(2,1)} %param.28) | copy-start | bytes 24580
  3.9 1.2 %copy-start.11 = (bf16[2,512,2,64]{1,3,2,0:T(8,128)(2,1)S(1)}, bf16[2,512,2,64]{1,3,2,0:T(8,128)(2,1)}, u32[]{:S(2)}) copy-start(bf16[2,512,2,64]{1,3,2,0:T(8,128)(2,1)} %param.27) | copy-start | bytes 786436
  6.0 1.5 %copy-start.13 = (f32[2,2,16,4]{2,3,1,0:T(4,128)S(1)}, f32[2,2,16,4]{2,3,1,0:T(4,128)}, u32[]{:S(2)}) copy-start(f32[2,2,16,4]{2,3,1,0:T(4,128)} %param.39) | copy-start | bytes 3076
  6.0 1.6 %copy-start.14 = (bf16[2,2,3,256]{3,1,2,0:T(2,128)(2,1)S(1)}, bf16[2,2,3,256]{3,1,2,0:T(2,128)(2,1)}, u32[]{:S(2)}) copy-start(bf16[2,2,3,256]{3,1,2,0:T(2,128)(2,1)} %param.36) | copy-start | bytes 18436
  6.0 1.7 %copy-start.15 = (bf16[2,2,3,2,64]{4,3,2,1,0:T(2,128)(2,1)S(1)}, bf16[2,2,3,2,64]{4,3,2,1,0:T(2,128)(2,1)}, u32[]{:S(2)}) copy-start(bf16[2,2,3,2,64]{4,3,2,1,0:T(2,128)(2,1)} %param.37) | copy-start | bytes 9220
  6.0 1.8 %copy-start.16 = (bf16[2,4,2,64]{3,2,1,0:T(2,128)(2,1)S(1)}, bf16[2,4,2,64]{3,2,1,0:T(2,128)(2,1)}, u32[]{:S(2)}) copy-start(bf16[2,4,2,64]{3,2,1,0:T(2,128)(2,1)} %param.30) | copy-start | bytes 6148
  6.0 1.9 %copy-start.17 = (bf16[2,4,256]{2,1,0:T(4,128)(2,1)S(1)}, bf16[2,4,256]{2,1,0:T(4,128)(2,1)}, u32[]{:S(2)}) copy-start(bf16[2,4,256]{2,1,0:T(4,128)(2,1)} %param.29) | copy-start | bytes 12292
  6.0 1.9 %copy-start.19 = (f32[2,4]{1,0:T(2,128)S(1)}, f32[2,4]{1,0:T(2,128)}, u32[]{:S(2)}) copy-start(f32[2,4]{1,0:T(2,128)} %param.33) | copy-start | bytes 100
  6.0 2.0 %copy-start.18 = (f32[2,256]{1,0:T(2,128)S(1)}, f32[2,256]{1,0:T(2,128)}, u32[]{:S(2)}) copy-start(f32[2,256]{1,0:T(2,128)} %param.34) | copy-start | bytes 6148
  6.0 2.0 %copy-start.20 = (f32[2,4]{1,0:T(2,128)S(1)}, f32[2,4]{1,0:T(2,128)}, u32[]{:S(2)}) copy-start(f32[2,4]{1,0:T(2,128)} %param.32) | copy-start | bytes 100
  6.1 2.0 %copy-start.21 = (f32[2,4]{1,0:T(2,128)S(1)}, f32[2,4]{1,0:T(2,128)}, u32[]{:S(2)}) copy-start(f32[2,4]{1,0:T(2,128)} %param.31) | copy-start | bytes 100
  6.1 2.0 %copy-start = (f32[2,2,4,64,128]{4,3,2,1,0:T(8,128)S(1)}, f32[2,2,4,64,128]{4,3,2,1,0:T(8,128)}, u32[]{:S(2)}) copy-start(f32[2,2,4,64,128]{4,3,2,1,0:T(8,128)} %param.38) | copy-start | bytes 1572868
  6.1 2.0 %copy-start.1 = (bf16[2,256,512]{2,1,0:T(8,128)(2,1)S(1)}, bf16[2,256,512]{2,1,0:T(8,128)(2,1)}, u32[]{:S(2)}) copy-start(bf16[2,256,512]{2,1,0:T(8,128)(2,1)} %wout.1) | copy-start | bytes 1572868
  6.1 2.0 %copy-start.7 = (bf16[128,128]{1,0:T(8,128)(2,1)S(1)}, bf16[128,128]{1,0:T(8,128)(2,1)}, u32[]{:S(2)}) copy-start(bf16[128,128]{1,0:T(8,128)(2,1)} %constant.17.clone.sel) | copy-start | bytes 98308
  6.1 2.0 %copy-start.8 = (f32[32,32]{1,0:T(8,128)S(1)}, f32[32,32]{1,0:T(8,128)}, u32[]{:S(2)}) copy-start(f32[32,32]{1,0:T(8,128)} %constant.19.clone.tri) | copy-start | bytes 12292
  6.1 2.0 %copy-start.9 = (f32[2,512]{1,0:T(2,128)S(1)}, f32[2,512]{1,0:T(2,128)}, u32[]{:S(2)}) copy-start(f32[2,512]{1,0:T(2,128)} %scale.1) | copy-start | bytes 12292
  6.1 2.0 %copy-start.10 = (s32[2]{0:T(128)S(1)}, s32[2]{0:T(128)}, u32[]{:S(2)}) copy-start(s32[2]{0:T(128)} %lens.1) | copy-start | bytes 28
  8.2 0.9 %copy-start.2 = (bf16[128,512]{1,0:T(8,128)(2,1)S(1)}, bf16[128,512]{1,0:T(8,128)(2,1)}, u32[]{:S(2)}) copy-start(bf16[128,512]{1,0:T(8,128)(2,1)} %x.7) | copy-start | bytes 393220
  9.1 0.9 %copy-start.3 = (bf16[256,256]{1,0:T(8,128)(2,1)S(1)}, bf16[256,256]{1,0:T(8,128)(2,1)}, u32[]{:S(2)}) copy-start(bf16[256,256]{1,0:T(8,128)(2,1)} %constant.18.clone.sel2) | copy-start | bytes 393220
  10.0 0.9 %copy-start.4 = (f32[128,256]{1,0:T(8,128)S(1)}, f32[128,256]{1,0:T(8,128)}, u32[]{:S(2)}) copy-start(f32[128,256]{1,0:T(8,128)} %constant.20.clone.ex) | copy-start | bytes 393220
  10.9 0.9 %copy-start.5 = (f32[256,128]{1,0:T(8,128)S(1)}, f32[256,128]{1,0:T(8,128)}, u32[]{:S(2)}) copy-start(f32[256,128]{1,0:T(8,128)} %constant.21.clone.ext) | copy-start | bytes 393220
  11.8 0.9 %copy-start.6 = (bf16[256,256]{1,0:T(8,128)(2,1)S(1)}, bf16[256,256]{1,0:T(8,128)(2,1)}, u32[]{:S(2)}) copy-start(bf16[256,256]{1,0:T(8,128)(2,1)} %constant.22.clone.ones) | copy-start | bytes 393220

commit v2 on v1

--- a/solution.py
+++ b/solution.py
@@ -2,7 +2,6 @@
 
 import jax
 import jax.numpy as jnp
-import numpy as np
 from jax import lax
 from jax.experimental import pallas as pl
 from jax.experimental.pallas import tpu as pltpu
@@ -11,7 +10,6 @@
 EPS = 1e-06
 LANES = 128
 FRONT = 8
-HIGHEST = lax.Precision.HIGHEST
 F32, BF16 = jnp.float32, jnp.bfloat16
 
 
@@ -19,23 +17,50 @@
     return -(-n // LANES) * LANES
 
 
-def dot(a, b, ca=1, cb=0, precision=None):
-    return lax.dot_general(
-        a, b, (((ca,), (cb,)), ((), ())), precision=precision, preferred_element_type=F32
+def dot(a, b, ca=1, cb=0):
+    return lax.dot_general(a, b, (((ca,), (cb,)), ((), ())), preferred_element_type=F32)
+
+
+def thirds(a):
+    high = a.astype(BF16)
+    rest = a - high.astype(F32)
+    middle = rest.astype(BF16)
+    return high, middle, (rest - middle.astype(F32)).astype(BF16)
+
+
+def grid(n_rows, n_cols):
+    return (
+        lax.broadcasted_iota(jnp.int32, (n_rows, n_cols), 0),
+        lax.broadcasted_iota(jnp.int32, (n_rows, n_cols), 1),
     )
+
+
+def over(a, n):
+    return lax.shift_right_logical(a, jnp.full_like(a, n.bit_length() - 1))
+
+
+def ones_where(cond):
+    return jnp.where(cond, 1.0, 0.0).astype(BF16)
+
+
+def far_first(k, me, n):
+    upper = me // (n // 2)
+    mirrored = n - 1 - me
+    return upper * (k + (k - me + n) // n) + (1 - upper) * (n - 1 - k - (k - mirrored + n) // n)
 
 
 def kernel(
     n_tp, n_dp, d_model, heads, groups, slots, seqs, hp_cols, map_cols,
-    lens, x, scale, w, taps, cache, par, hv, extra, state, wout, sel, sel2, tri, ex, ext, ones,
+    lens, x, scale, w_pair, w_maps, w_step, tap_u, tap_m, bias, rate, skip, gain, cache_u, cache_m, extra_t,
+    state_hbm, wout_hbm,
     stream, kept, ssm,
-    a_send, a_recv, m_send, m_recv, h_send, h_recv, o_send, o_recv, n_send, n_recv, padded,
-    a_ss, a_rs, m_ss, m_rs, h_ss, h_rs, o_ss, o_rs, n_ss, n_rs,
+    a_send, a_recv, m_send, m_recv, h_send, h_recv, o_send, o_recv, n_send, n_recv, padded, step_w, state, wout, taps, par, extra,
+    a_ss, a_rs, m_ss, m_rs, h_ss, h_rs, o_ss, o_rs, n_ss, n_rs, s_sem, w_sem,
 ):
     tp, dp = lax.axis_index("tp"), lax.axis_index("dp")
-    layers = w.shape[0]
+    layers = w_pair.shape[0]
     rows = seqs * slots
-    taps_n = taps.shape[1]
+    taps_n = tap_u.shape[1]
     keep = taps_n - 1
     zc = up(hp_cols)
     ng = map_cols // groups
@@ -44,6 +69,10 @@
     per = rows // cut
     head_size = hp_cols // heads
 
+    state_copy = pltpu.make_async_copy(state_hbm, state, s_sem)
+    wout_copy = pltpu.make_async_copy(wout_hbm, wout, w_sem)
+    state_copy.start()
+    wout_copy.start()
     barrier = pltpu.get_barrier_semaphore()
     for k in range(1, n_dp):
         pl.semaphore_signal(barrier, inc=1, device_id={"dp": lax.rem(dp + k, n_dp)})
@@ -54,10 +83,42 @@
     slot = lax.broadcasted_iota(jnp.int32, (slots, 1), 0)
     mask = jnp.concatenate([(slot < lens[s]).astype(F32) for s in range(seqs)], axis=0)
     lane = lax.broadcasted_iota(jnp.int32, (1, LANES), 1)
-    r_id = lax.broadcasted_iota(jnp.int32, (rows, rows), 0)
-    c_id = lax.broadcasted_iota(jnp.int32, (rows, rows), 1)
-    causal = tri[...] > 0.5
+    r, c = grid(rows, rows)
+    causal = (over(r, slots) == over(c, slots)) & (c <= r)
+    tri = ones_where(causal)
+    r, c = grid(2 * map_cols, up(2 * map_cols))
+    which = over(r, ng) & 1
+    sel = ones_where(c == which * map_cols + groups * (r & (ng - 1)) + over(r, 2 * ng))
+    r, c = grid(n_tp * 2 * ng, 2 * n_state)
+    sel2 = ones_where(c == (over(r, ng) & 1) * n_state + over(r, 2 * ng) * ng + (r & (ng - 1)))
+    r, c = grid(LANES, hp_cols)
+    ex = ones_where(r == over(c, head_size))
+    r, c = grid(hp_cols, LANES)
+    ext = ones_where(c == over(r, head_size))
+    r, c = grid(hp_cols, hp_cols)
+    ones = ones_where(over(r, head_size) == over(c, head_size))
+    r, c = grid(LANES, 2 * LANES)
+    spread = ones_where(c == 2 * r)
     padded[...] = jnp.zeros_like(padded)
+    step_w[...] = jnp.zeros_like(step_w)
+    taps[...] = jnp.zeros_like(taps)
+    par[...] = jnp.zeros_like(par)
+    extra[...] = jnp.zeros_like(extra)
+    for l in range(layers):
+        step_w[l, :heads, :] = w_step[l]
+        taps[l, :taps_n, :hp_cols] = tap_u[l].astype(F32)
+        for t in range(taps_n):
+            pair = tap_m[l, t].astype(F32)
+            for which in range(2):
+                at = zc + which * map_cols
+                taps[l, t : t + 1, at : at + map_cols] = pair[which : which + 1]
+        par[l, 0:1, :heads] = bias[l : l + 1, :]
+        par[l, 1:2, :heads] = rate[l : l + 1, :]
+        par[l, 2:3, :heads] = skip[l : l + 1, :]
+        for s in range(seqs):
+            extra[l, :heads, s * slots : (s + 1) * slots] = extra_t[l, s]
+    extra_rows = [extra[l].T[:rows] for l in range(layers)]
+    skip_x = [sum(dot(piece, ex) for piece in thirds(par[l]))[2:3] for l in range(layers)]
     sends = []
 
     def copy(src, dst, ss, rs, where):
@@ -69,11 +130,18 @@
         st = stream[...]
         squares = jnp.sum(st * st, axis=1, keepdims=True)
         normed = (st * scale[l : l + 1, :]).astype(BF16)
-        part = dot(normed, w[l])
-        tail = part[:, part.shape[1] - LANES :]
+        even = jnp.concatenate(
+            [dot(normed[:, i : i + LANES], spread) for i in range(0, normed.shape[1], LANES)], axis=1
+        )
+        odd = pltpu.roll(even, 1, 1)
+        pair = dot(jnp.concatenate([even.astype(BF16), odd.astype(BF16)], axis=0), w_pair[l])
+        tokens = st.shape[0]
+        tail = dot(normed, step_w[l], 1, 1)
         high = squares.astype(BF16).astype(F32)
         tail = jnp.where(lane == LANES - 2, high, jnp.where(lane == LANES - 1, squares - high, tail))
-        part = jnp.concatenate([part[:, : part.shape[1] - LANES], tail], axis=1).astype(BF16)
+        part = jnp.concatenate(
+            [pair[:tokens], pair[tokens:], dot(normed, w_maps[l], 1, 1), tail], axis=1
+        ).astype(BF16)
         for b in range(n_dp):
             a_send[l, b] = part[b * rows : (b + 1) * rows]
         if l == 0:
@@ -97,7 +165,13 @@
         conv_w = taps.shape[2]
         pieces = []
         for s in range(seqs):
-            padded[s, FRONT - keep : FRONT, :] = cache[l, s].astype(F32)
+            for t in range(keep):
+                at = FRONT - keep + t
+                padded[s, at : at + 1, :hp_cols] = cache_u[l, t].astype(F32)[s : s + 1]
+                pair = cache_m[l, s, t].astype(F32)
+                for which in range(2):
+                    col = zc + which * map_cols
+                    padded[s, at : at + 1, col : col + map_cols] = pair[which : which + 1]
             padded[s, FRONT : FRONT + slots, :] = proj[s * slots : (s + 1) * slots, zc : zc + conv_w]
             total = padded[s, FRONT - keep : FRONT - keep + slots, :] * taps[l, 0:1, :]
             for t in range(1, taps_n):
@@ -107,7 +181,7 @@
         filtered = jnp.concatenate(pieces, axis=0)
         filtered = filtered * jax.nn.sigmoid(filtered)
         maps = filtered[:, conv_w - up(2 * map_cols) :].astype(BF16)
-        sorted_maps = dot(sel[...], maps, 1, 1)
+        sorted_maps = dot(sel, maps, 1, 1)
         for g in range(groups):
             m_send[l, g] = sorted_maps[g * 2 * ng : (g + 1) * 2 * ng, :].astype(BF16)
 
@@ -115,12 +189,11 @@
             return rank * heads // (heads * n_tp // groups)
 
         flights = []
-        for k in range(1, n_tp):
-            to = lax.rem(tp + k, n_tp)
-            c = copy(m_send.at[l, group_of(to)], m_recv.at[l, tp], m_ss.at[l, k - 1], m_rs.at[l, k - 1], {"tp": to})
+        for k in range(n_tp - 1):
+            to = far_first(k, tp, n_tp)
+            c = copy(m_send.at[l, group_of(to)], m_recv.at[l, tp], m_ss.at[l, k], m_rs.at[l, tp], {"tp": to})
             c.start()
-            flights.append(c)
-        sends += flights
+            sends.append(c)
         m_recv[l, tp] = m_send[l, group_of(tp)]
 
         for s in range(seqs):
@@ -131,13 +204,16 @@
         raw = proj[:, proj.shape[1] - LANES :] + par[l, 0:1, :]
         step = (jnp.maximum(raw, 0.0) + jnp.log1p(jnp.exp(-jnp.abs(raw)))) * mask
         step = jnp.where(lane < heads, step, 0.0)
-        logdec = extra[l] * mask - step * jnp.exp(par[l, 1:2, :])
+        logdec = extra_rows[l] * mask - step * jnp.exp(par[l, 1:2, :])
         logdec = jnp.where(lane < heads, logdec, 0.0)
-        sums = dot(tri[...], logdec, precision=HIGHEST)
+        parts = dot(tri, jnp.concatenate(thirds(logdec), axis=1))
+        sums = parts[:, :LANES] + parts[:, LANES : 2 * LANES] + parts[:, 2 * LANES :]
         sums_t = sums.T
         step_t = step.T
-        both = dot(jnp.concatenate([sums, step], axis=0), ex[...], precision=HIGHEST)
-        sums_x, step_x = both[:rows], both[rows:]
+        sums_parts, step_parts = thirds(sums), thirds(step)
+        both = dot(jnp.concatenate(sums_parts + step_parts, axis=0), ex)
+        sums_x = both[:rows] + both[rows : 2 * rows] + both[2 * rows : 3 * rows]
+        step_x = both[3 * rows : 4 * rows] + both[4 * rows : 5 * rows] + both[5 * rows :]
         inp = filtered[:, :hp_cols]
         gate = proj[:, :hp_cols]
         last_x = jnp.concatenate(
@@ -150,18 +226,22 @@
         weighted = (jnp.exp(last_x - sums_x) * step_x * inp).astype(BF16)
         inp_b = inp.astype(BF16)
         grow = jnp.exp(sums_x)
-        direct = hv[l, 0:1, :] * inp
+        direct = skip_x[l] * inp
         gate = gate * jax.nn.sigmoid(gate)
-        rows_sum = dot(ext[...], sums, 1, 1, precision=HIGHEST)
+        rows_sum = sum(dot(ext, piece, 1, 1) for piece in sums_parts)
         segs = []
         for h in range(heads):
             gap = sums[:, h : h + 1] - sums_t[h : h + 1, :]
             segs.append(jnp.exp(jnp.where(causal, gap, -jnp.inf)) * step_t[h : h + 1, :])
 
-        for c in flights:
-            c.wait_recv()
+        if l == 0:
+            state_copy.wait()
+            wout_copy.wait()
+        for k in range(1, n_tp):
+            src = lax.rem(tp + n_tp - k, n_tp)
+            copy(m_send.at[l, 0], m_recv.at[l, src], m_ss.at[l, 0], m_rs.at[l, src], {"tp": src}).wait_recv()
         got = m_recv[l].astype(F32).reshape(n_tp * 2 * ng, rows)
-        both_maps = dot(got.T.astype(BF16), sel2[...]).astype(BF16)
+        both_maps = dot(got.T.astype(BF16), sel2).astype(BF16)
         b_map, c_map = both_maps[:, :n_state], both_maps[:, n_state:]
         cross = dot(c_map, b_map, 1, 1)
         within = jnp.concatenate(
@@ -182,8 +262,8 @@
         power = read * read
         p_hi = power.astype(BF16)
         p_lo = (power - p_hi.astype(F32)).astype(BF16)
-        mean = (dot(p_hi, ones[...]) + dot(p_lo, ones[...])) / head_size
-        headout = (read * lax.rsqrt(mean + EPS) * hv[l, 1:2, :] * mask).astype(BF16)
+        mean = (dot(p_hi, ones) + dot(p_lo, ones)) / head_size
+        headout = (read * lax.rsqrt(mean + EPS) * gain[l : l + 1, :] * mask).astype(BF16)
         h_send[l] = headout
         flights = []
         for k in range(1, n_dp):
@@ -220,15 +300,14 @@
         fresh = total.astype(BF16)
         n_send[l] = fresh
         n_recv[l, tp] = fresh
-        flights = []
+        for k in range(n_tp - 1):
+            to = far_first(k, tp, n_tp)
+            c = copy(n_send.at[l], n_recv.at[l, tp], n_ss.at[l, k], n_rs.at[l, tp], {"tp": to})
+            c.start()
+            sends.append(c)
         for k in range(1, n_tp):
-            to = lax.rem(tp + k, n_tp)
-            c = copy(n_send.at[l], n_recv.at[l, tp], n_ss.at[l, k - 1], n_rs.at[l, k - 1], {"tp": to})
-            c.start()
-            flights.append(c)
-        sends += flights
-        for c in flights:
-            c.wait_recv()
+            src = lax.rem(tp + n_tp - k, n_tp)
+            copy(n_send.at[l], n_recv.at[l, src], n_ss.at[l, 0], n_rs.at[l, src], {"tp": src}).wait_recv()
         stream[...] += n_recv[l].astype(F32).reshape(stream.shape)
 
     for c in sends:
@@ -260,55 +339,24 @@
         pad = up(a.shape[-1]) - a.shape[-1]
         return a if pad == 0 else jnp.pad(a, [(0, 0)] * (a.ndim - 1) + [(0, pad)])
 
-    w = jnp.concatenate(
-        [
-            wide(gate_input_weight[:, :, 0]),
-            wide(gate_input_weight[:, :, 1]),
-            wide(maps_weight.reshape(layers, d_here, 2 * map_cols)),
-            wide(step_weight),
-        ],
-        axis=2,
-    )
-    taps = jnp.concatenate(
-        [wide(input_tap_weight), wide(map_tap_weight.reshape(layers, -1, 2 * map_cols))], axis=2
-    ).astype(F32)
-    cache = jnp.concatenate(
-        [
-            wide(convolution_input_cache),
-            wide(convolution_map_cache.reshape(layers, seqs, keep, 2 * map_cols)),
-        ],
-        axis=3,
-    )
-    par = wide(jnp.stack([step_size_bias, decay_rate_logarithm], axis=1))
-    hv = jnp.stack([jnp.repeat(direct_path_weight, head_size, axis=1), head_norm_scale], axis=1)
-    extra = wide(extra_log_decay.reshape(layers, rows, heads))
+    w_pair = wide(gate_input_weight.reshape(layers, 2 * d_here, hp_cols))
+    w_maps = jnp.transpose(maps_weight, (0, 2, 3, 1)).reshape(layers, 2 * map_cols, d_here)
+    if up(2 * map_cols) > 2 * map_cols:
+        w_maps = jnp.pad(w_maps, ((0, 0), (0, up(2 * map_cols) - 2 * map_cols), (0, 0)))
+    w_step = jnp.transpose(step_weight, (0, 2, 1))
+    cache_u = jnp.transpose(convolution_input_cache, (0, 2, 1, 3))
+    extra_t = jnp.transpose(extra_log_decay, (0, 1, 3, 2))
     state = recurrent_state.reshape(layers, seqs, hp_cols, n_state)
 
-    sel = np.zeros((2 * map_cols, up(2 * map_cols)), np.float32)
-    for g in range(groups):
-        for which in range(2):
-            for j in range(ng):
-                sel[g * 2 * ng + which * ng + j, which * map_cols + groups * j + g] = 1
-    sel2 = np.zeros((n_tp * 2 * ng, 2 * n_state), np.float32)
-    for src in range(n_tp):
-        for which in range(2):
-            for j in range(ng):
-                sel2[src * 2 * ng + which * ng + j, which * n_state + src * ng + j] = 1
-    tri = np.kron(np.eye(seqs), np.tril(np.ones((slots, slots)))).astype(np.float32)
-    ex = np.zeros((LANES, hp_cols), np.float32)
-    ex[:heads] = np.kron(np.eye(heads), np.ones((1, head_size)))
-    ones = np.kron(np.eye(heads), np.ones((head_size, head_size))).astype(np.float32)
-
     vmem = pl.BlockSpec(memory_space=pltpu.VMEM)
-    wide_cols = w.shape[2]
-    conv_w = taps.shape[2]
+    wide_cols = 2 * up(hp_cols) + up(2 * map_cols) + LANES
+    anywhere = pl.BlockSpec(memory_space=pl.ANY)
+    conv_w = up(hp_cols) + up(2 * map_cols)
     cut = tokens.shape[0] // n_tp
     sems = lambda n: pltpu.SemaphoreType.DMA((layers, n))
-    args = [
-        tokens, input_norm_scale, w, taps, cache, par, hv, extra, state, output_weight,
-        jnp.asarray(sel, BF16), jnp.asarray(sel2, BF16), jnp.asarray(tri), jnp.asarray(ex),
-        jnp.asarray(ex.T.copy()), jnp.asarray(ones, BF16),
-    ]
+    args = [tokens, input_norm_scale, w_pair, w_maps, w_step, input_tap_weight,
+        map_tap_weight, step_size_bias, decay_rate_logarithm, direct_path_weight, head_norm_scale,
+        cache_u, convolution_map_cache, extra_t]
     stream, kept, ssm = pl.pallas_call(
         functools.partial(
             kernel, n_tp, n_dp, d_here * n_dp, heads, groups, slots, seqs, hp_cols, map_cols
@@ -318,7 +366,7 @@
             jax.ShapeDtypeStruct((layers, seqs, 8, conv_w), BF16),
             jax.ShapeDtypeStruct(state.shape, F32),
         ),
-        in_specs=[pl.BlockSpec(memory_space=pltpu.SMEM)] + [vmem] * len(args),
+        in_specs=[pl.BlockSpec(memory_space=pltpu.SMEM)] + [vmem] * len(args) + [anywhere] * 2,
         out_specs=(vmem, vmem, vmem),
         scratch_shapes=[
             pltpu.VMEM((layers, n_dp, rows, wide_cols), BF16),
@@ -332,14 +380,21 @@
             pltpu.VMEM((layers, cut, d_here), BF16),
             pltpu.VMEM((layers, n_tp, cut, d_here), BF16),
             pltpu.VMEM((seqs, FRONT + slots, conv_w), F32),
-            sems(n_dp - 1), sems(n_dp - 1), sems(n_tp - 1), sems(n_tp - 1), sems(n_dp - 1),
-            sems(n_dp - 1), sems(n_tp), sems(n_tp), sems(n_tp - 1), sems(n_tp - 1),
+            pltpu.VMEM((layers, LANES, d_here), BF16),
+            pltpu.VMEM(state.shape, F32),
+            pltpu.VMEM(output_weight.shape, BF16),
+            pltpu.VMEM((layers, 8, conv_w), F32),
+            pltpu.VMEM((layers, 8, LANES), F32),
+            pltpu.VMEM((layers, LANES, LANES), F32),
+            sems(n_dp - 1), sems(n_dp - 1), sems(n_tp - 1), sems(n_tp), sems(n_dp - 1),
+            sems(n_dp - 1), sems(n_tp), sems(n_tp), sems(n_tp - 1), sems(n_tp),
+            pltpu.SemaphoreType.DMA, pltpu.SemaphoreType.DMA,
         ],
         compiler_params=pltpu.CompilerParams(
             collective_id=0, has_side_effects=True, vmem_limit_bytes=48 * 2**20
         ),
         name="mixer",
-    )(lengths, *args)
+    )(lengths, *args, state, output_weight)
     conv_in = kept[:, :, :keep, :hp_cols]
     start = conv_w - up(2 * map_cols)
     conv_maps = kept[:, :, :keep, start : start + 2 * map_cols].reshape(

time: 65.3 us -> 54.5 us (0.83)
  local copies, waits for them, and re-layouts: 13.2 us -> 4.4 us
  other arithmetic: 1.41 us -> 0 us
    unnamed x50 -> x35, local copies, waits for them, and re-layouts: 7.01 us -> 2.16 us
    slice x1 -> x0, local copies, waits for them, and re-layouts: 3.27 us -> none  [body(): gate_input_weight[:, :, 0]]
    concatenate x2 -> x0, other arithmetic: 1.39 us -> none  [the longest x1 1.38 us: body(): jnp.concatenate([wide(gate_input_weight[:, :, 0]), wide(gate_input_weight...]
    squeeze x1 -> x0, local copies, waits for them, and re-layouts: 1 us -> none  [body(): gate_input_weight[:, :, 1]]
    reshape x3 -> x1, local copies, waits for them, and re-layouts: 1.01 us -> 1.55 us  [body(): w_pair = wide(gate_input_weight.reshape(layers, 2 * d_here, hp_cols))]
where the time goes in v2:
time: 54.5 us; the launch traced here: 54.4 us
  Pallas kernels  49.1 us (90%)
  local copies, waits for them, and re-layouts  4.4 us (8%)
  between operations  0.92 us (2%)
    pallas_call x1, Pallas kernels, body(): pl.pallas_call(functools.partial(kernel, n_tp, n_dp, d_here * n_dp, heads...  49.1 us
    unnamed x35, local copies, waits for them, and re-layouts  2.16 us
    reshape x1, local copies, waits for them, and re-layouts, body(): w_pair = wide(gate_input_weight.reshape(layers, 2 * d_here, hp_cols))  1.55 us

profile of v2, /device:TPU:0, one launch (start us, length us, event | category | flops | bytes accessed | tf_op | source)
XLA Modules:
  0.0 54.4 jit_solution(1157446357131992755)
XLA Ops:
  0.6 0.0 copy-start
  0.6 0.0 copy-start.1
  0.7 0.0 copy-start.2
  0.7 0.0 copy-start.3
  0.7 0.0 copy-start.4
  0.7 0.0 copy-start.5
  0.7 0.0 copy-start.6
  0.7 0.0 copy-start.7
  0.7 0.0 copy-start.8
  0.7 0.0 copy-start.9
  0.7 0.0 copy-start.10
  0.7 0.0 copy-start.11
  0.8 0.0 copy-start.12
  0.8 0.0 copy-start.13
  0.8 0.0 copy-start.14
  0.8 0.0 copy-start.15
  0.8 1.5 %reshape.23.w_pair = bf16[2,1024,256]{2,1,0:T(8,128)(2,1)S(1)} reshape(bf16[2,512,2,256]{3,2,1,0:T(2,128)(2,1)} %param.20) | data formatting | bytes 2097152 | tf_op jit(solution)/shard_map/reshape | solution.py:342
  2.4 0.0 copy-done
  2.4 0.0 copy-done.1
  2.4 0.0 copy-done.2
  2.4 0.0 copy-done.3
  2.4 0.0 copy-done.4
  2.4 0.0 copy-done.5
  2.4 0.0 copy-done.6
  2.4 0.0 copy-done.7
  2.4 0.0 copy-done.8
  2.4 0.0 copy-done.9
  2.5 0.0 copy-done.10
  2.5 0.0 copy-done.11
  2.5 0.0 copy-done.12
  2.5 0.0 copy-done.13
  2.5 0.0 copy-done.14
  2.5 0.0 copy-done.15
  2.5 49.1 %mixer.1 = (f32[128,512]{1,0:T(8,128)S(1)}, bf16[2,2,8,384]{3,2,1,0:T(8,128)(2,1)S(1)}, f32[2,2,256,128]{3,2,1,0:T(8,128)S(1)}) custom-call(s32[2]{0:T(128)S(1)} %copy-done.15, bf16[128,512]{1,0:T(8,128)(2,1)S(1)} %copy-done.3, f32[2,512]{1,0:T(2,128)S(1)} %copy-done.8, bf16[2,1024,256]{2,1,0:T(8,128)(2,1)S(1)} %reshape.23.w_pair, ...), custom_call_target="tpu_custom_call" | custom-call | tf_op jit(solution)/shard_map/mixer/pallas_call | solution.py:360
  51.6 0.6 %copy.23 = bf16[2,2,3,256]{3,1,2,0:T(2,128)(2,1)} copy(bf16[2,2,3,256]{3,2,1,0:T(4,128)(2,1)S(1)} %slice.6) | data formatting | bytes 12288
  52.2 0.7 %reshape.28 = bf16[2,2,3,2,64]{4,3,2,1,0:T(2,128)(2,1)} reshape(bf16[2,2,3,128]{3,2,1,0:T(4,128)(2,1)S(1)} %slice.7) | data formatting | bytes 6144 | tf_op jit(solution)/shard_map/reshape | solution.py:400
  52.9 0.7 %copy.28 = f32[128,512]{1,0:T(8,128)} copy(f32[128,512]{1,0:T(8,128)S(1)} %get-tuple-element.22) | data formatting | bytes 524288
  53.6 0.8 %copy.29 = f32[2,2,4,64,128]{4,3,2,1,0:T(8,128)} copy(f32[2,2,4,64,128]{4,3,2,1,0:T(8,128)S(1)} %bitcast.9) | data formatting | bytes 1048576
  (2 shorter events, 0.0 us)
Async XLA Ops:
  0.6 1.7 %copy-start = (f32[2,2,4,64,128]{4,3,2,1,0:T(8,128)S(1)}, f32[2,2,4,64,128]{4,3,2,1,0:T(8,128)}, u32[]{:S(2)}) copy-start(f32[2,2,4,64,128]{4,3,2,1,0:T(8,128)} %param.32) | copy-start | bytes 1572868
  0.6 1.7 %copy-start.1 = (bf16[2,256,512]{2,1,0:T(8,128)(2,1)S(1)}, bf16[2,256,512]{2,1,0:T(8,128)(2,1)}, u32[]{:S(2)}) copy-start(bf16[2,256,512]{2,1,0:T(8,128)(2,1)} %wout_hbm.1) | copy-start | bytes 1572868
  0.7 1.7 %copy-start.2 = (bf16[2,512,2,64]{1,3,2,0:T(8,128)(2,1)S(1)}, bf16[2,512,2,64]{1,3,2,0:T(8,128)(2,1)}, u32[]{:S(2)}) copy-start(bf16[2,512,2,64]{1,3,2,0:T(8,128)(2,1)} %param.21) | copy-start | bytes 786436
  0.7 1.7 %copy-start.3 = (bf16[128,512]{1,0:T(8,128)(2,1)S(1)}, bf16[128,512]{1,0:T(8,128)(2,1)}, u32[]{:S(2)}) copy-start(bf16[128,512]{1,0:T(8,128)(2,1)} %x.1) | copy-start | bytes 393220
  0.7 1.7 %copy-start.4 = (bf16[2,512,4]{1,2,0:T(4,128)(2,1)S(1)}, bf16[2,512,4]{1,2,0:T(4,128)(2,1)}, u32[]{:S(2)}) copy-start(bf16[2,512,4]{1,2,0:T(4,128)(2,1)} %param.22) | copy-start | bytes 24580
  0.7 1.7 %copy-start.5 = (f32[2,2,16,4]{2,3,1,0:T(4,128)S(1)}, f32[2,2,16,4]{2,3,1,0:T(4,128)}, u32[]{:S(2)}) copy-start(f32[2,2,16,4]{2,3,1,0:T(4,128)} %param.33) | copy-start | bytes 3076
  0.7 1.7 %copy-start.6 = (bf16[2,2,3,256]{3,1,2,0:T(2,128)(2,1)S(1)}, bf16[2,2,3,256]{3,1,2,0:T(2,128)(2,1)}, u32[]{:S(2)}) copy-start(bf16[2,2,3,256]{3,1,2,0:T(2,128)(2,1)} %param.30) | copy-start | bytes 18436
  0.7 1.7 %copy-start.7 = (bf16[2,2,3,2,64]{4,3,2,1,0:T(2,128)(2,1)S(1)}, bf16[2,2,3,2,64]{4,3,2,1,0:T(2,128)(2,1)}, u32[]{:S(2)}) copy-start(bf16[2,2,3,2,64]{4,3,2,1,0:T(2,128)(2,1)} %cache_m.1) | copy-start | bytes 9220
  0.7 1.7 %copy-start.8 = (f32[2,512]{1,0:T(2,128)S(1)}, f32[2,512]{1,0:T(2,128)}, u32[]{:S(2)}) copy-start(f32[2,512]{1,0:T(2,128)} %scale.1) | copy-start | bytes 12292
  0.7 1.7 %copy-start.9 = (bf16[2,4,256]{2,1,0:T(4,128)(2,1)S(1)}, bf16[2,4,256]{2,1,0:T(4,128)(2,1)}, u32[]{:S(2)}) copy-start(bf16[2,4,256]{2,1,0:T(4,128)(2,1)} %tap_u.1) | copy-start | bytes 12292
  0.7 1.7 %copy-start.10 = (bf16[2,4,2,64]{3,2,1,0:T(2,128)(2,1)S(1)}, bf16[2,4,2,64]{3,2,1,0:T(2,128)(2,1)}, u32[]{:S(2)}) copy-start(bf16[2,4,2,64]{3,2,1,0:T(2,128)(2,1)} %tap_m.1) | copy-start | bytes 6148
  0.7 1.7 %copy-start.11 = (f32[2,256]{1,0:T(2,128)S(1)}, f32[2,256]{1,0:T(2,128)}, u32[]{:S(2)}) copy-start(f32[2,256]{1,0:T(2,128)} %gain.1) | copy-start | bytes 6148
  0.8 1.7 %copy-start.12 = (f32[2,4]{1,0:T(2,128)S(1)}, f32[2,4]{1,0:T(2,128)}, u32[]{:S(2)}) copy-start(f32[2,4]{1,0:T(2,128)} %bias.1) | copy-start | bytes 100
  0.8 1.7 %copy-start.13 = (f32[2,4]{1,0:T(2,128)S(1)}, f32[2,4]{1,0:T(2,128)}, u32[]{:S(2)}) copy-start(f32[2,4]{1,0:T(2,128)} %rate.1) | copy-start | bytes 100
  0.8 1.7 %copy-start.14 = (f32[2,4]{1,0:T(2,128)S(1)}, f32[2,4]{1,0:T(2,128)}, u32[]{:S(2)}) copy-start(f32[2,4]{1,0:T(2,128)} %skip.1) | copy-start | bytes 100
  0.8 1.7 %copy-start.15 = (s32[2]{0:T(128)S(1)}, s32[2]{0:T(128)}, u32[]{:S(2)}) copy-start(s32[2]{0:T(128)} %lens.1) | copy-start | bytes 28
